TPU v7x, 256 devices: a whole 4x4x8 slice. The times are simulated.
256 devices in a mesh: sp: 128 (over z, y, x), tp: 2 (over core).
Axes of the slice: x: 4, y: 4, z: 8, core: 2. Of those that a mesh axis runs over, the one named last changes fastest.
Arguments:
- queries: bfloat16 [196608, 1024], P('sp', 'tp'), may hold values from -6 to 6
- forget_logit: bfloat16 [196608, 1024], P('sp', 'tp'), may hold values from -8 to 8
- value_rows: bfloat16 [196608, 1024], P('sp', 'tp'), may hold values from -10 to 10
- out_gate: bfloat16 [196608, 1024], P('sp', 'tp'), may hold values from -6 to 6
- floor_gap: float32 [1024], P('tp'), may hold values from 0 to 0.1, as said below
- head_gain: float32 [1024], P('tp'), may hold values from 0.1 to 1.9
- state_in: float32 [8, 128, 128], P('tp'), may hold values from -0.625 to 0.625
- out_weight: bfloat16 [1024, 2048], P('tp'), may hold values from -0.1875 to 0.1875
Outputs:
- projected: bfloat16 [196608, 2048], P(('sp', 'tp'))
- state_out: float32 [8, 16384], P('tp', 'sp')
Inputs may be any that keep to these rules, and one draw needn't show every extreme that they name: `floor_gap`: strictly between 0 and 0.1.
All inputs are finite; a program needn't handle non-finite values.
Results may differ from a plain program's by a relative error of at most 0.009.
Values may be sent and summed in bfloat16 or wider, within the bound.
No kernel may reach another device: no remote copies, remote signals or barrier semaphores. Data moves between devices by JAX's collectives and lax.ppermute only.
A program may use at most 128 MiB of HBM per device.

v0:
```python
import jax
import jax.numpy as jnp
from jax import lax
from jax.sharding import Mesh
from jax.sharding import PartitionSpec as P

BLOCK = 128
SP = ("sp_0", "sp_1", "sp_2")
SP_TP = ("sp_0", "sp_1", "sp_2", "tp")
epsilon = 1e-06


def neutral_like(value, identity):
    return jax.tree.map(
        lambda a, e: jnp.broadcast_to(jnp.asarray(e, a.dtype), a.shape), value, identity
    )


def entering(value, axes, combine, identity):
    before = start = neutral_like(value, identity)
    so_far = value
    for axis in reversed(axes):
        length, mine = (lax.axis_size(axis), lax.axis_index(axis))
        pieces = jax.tree.map(lambda part: lax.all_gather(part, axis), so_far)
        inside, so_far = (start, start)
        for k in range(length):
            passed = k < mine
            so_far = combine(so_far, jax.tree.map(lambda part: part[k], pieces))
            inside = jax.tree.map(lambda new, old: jnp.where(passed, new, old), so_far, inside)
        before = combine(inside, before)
    return before


def broadcast_by_axis(value, axes, root):
    value = jnp.where(lax.axis_index(axes) == root, value, jnp.zeros_like(value))
    for axis in axes:
        value = lax.psum(value, axis)
    return value


def to_blocks(values, head_count):
    blocks = values.shape[0] // BLOCK
    return values.reshape(blocks, BLOCK, head_count, values.shape[1] // head_count)


def join_state(earlier, later):
    return (earlier[0] * later[0], later[0][..., None] * earlier[1] + later[1])


def per_device(
    queries, forget_logit, value_rows, out_gate, floor_gap, head_gain, state_in, out_weight
):
    span_rows = queries.shape[0]
    head_count = state_in.shape[0]
    key_gate = to_blocks(floor_gap * jax.nn.sigmoid(-forget_logit.astype(jnp.float32)), head_count)
    log_forget = jnp.log1p(-key_gate)
    reader = to_blocks(jax.nn.silu(queries.astype(jnp.float32)), head_count)
    written_update = to_blocks(value_rows.astype(jnp.float32), head_count)
    positions = jnp.arange(BLOCK)
    causal = positions[:, None] >= positions[None, :]
    lower_ones = causal.astype(jnp.float32)
    cumul = jnp.einsum("cs,nshk->nchk", lower_ones, log_forget)
    scaled_readout = reader * jnp.exp(cumul)
    key_scaled = key_gate * jnp.exp(-cumul)
    scores = jnp.einsum("nchk,nshk->nhcs", scaled_readout, key_scaled)
    scores = jnp.where(causal, scores, 0.0)
    within = jnp.einsum("nhcs,nshv->nchv", scores, written_update)
    block_log_decay = cumul[:, -1]
    decay_to_finish = key_gate * jnp.exp(block_log_decay[:, None] - cumul)
    segment_state = jnp.einsum("nshk,nshv->nhkv", decay_to_finish, written_update)
    block_final_rows = jnp.cumsum(block_log_decay, axis=0)
    starts = block_final_rows - block_log_decay
    overall_log_decay = block_final_rows[-1]
    block_ids = jnp.arange(block_final_rows.shape[0])
    earlier_mask = (block_ids[:, None] > block_ids[None, :])[:, :, None, None]
    spacing = jnp.where(earlier_mask, starts[:, None] - block_final_rows[None, :], 0.0)
    carry_weight = jnp.where(earlier_mask, jnp.exp(spacing), 0.0)
    local_before = jnp.einsum("jihk,ihkv->jhkv", carry_weight, segment_state)
    decay_dev = jnp.exp(overall_log_decay)
    state_dev = jnp.einsum(
        "lpt,lptr->ptr", jnp.exp(overall_log_decay[None] - block_final_rows), segment_state
    )
    prefix_decay, prefix_state = entering(
        (decay_dev, state_dev),
        SP,
        join_state,
        (jnp.ones_like(decay_dev), jnp.zeros_like(state_dev)),
    )
    incoming = prefix_decay[..., None] * state_in + prefix_state
    before = local_before + jnp.exp(starts)[..., None] * incoming[None]
    unscaled_output = within + jnp.einsum("nchk,nhkv->nchv", scaled_readout, before)
    mean_square = jnp.mean(unscaled_output * unscaled_output, axis=-1, keepdims=True)
    gain_rows = head_gain.reshape(head_count, -1)
    normed = unscaled_output * lax.rsqrt(mean_square + epsilon) * gain_rows
    gating = jax.nn.silu(to_blocks(out_gate.astype(jnp.float32), head_count))
    gated = (normed * gating).astype(jnp.bfloat16).reshape(span_rows, -1)
    regrouped = lax.all_to_all(gated, "tp", split_axis=0, concat_axis=1, tiled=True)
    summed = jnp.dot(
        regrouped,
        lax.all_gather(out_weight, "tp", axis=0, tiled=True),
        preferred_element_type=jnp.float32,
    )
    projected = summed.astype(jnp.bfloat16)
    finished = (decay_dev[..., None] * incoming + state_dev).reshape(head_count, -1)
    whole_final = broadcast_by_axis(
        finished.astype(jnp.bfloat16), SP, lax.axis_size(SP) - 1
    ).astype(finished.dtype)
    share = whole_final.shape[1] // lax.axis_size(SP)
    offset = lax.axis_index(SP) * share
    state_out = lax.dynamic_slice_in_dim(whole_final, offset, share, 1)
    return (projected, state_out)


def solution(mesh):
    torus = Mesh(mesh.devices.reshape(8, 4, 4, mesh.shape["tp"]), ("sp_0", "sp_1", "sp_2", "tp"))
    placed = (
        P(SP, "tp"),
        P(SP, "tp"),
        P(SP, "tp"),
        P(SP, "tp"),
        P("tp"),
        P("tp"),
        P("tp", None, None),
        P("tp", None),
    )
    return jax.shard_map(
        per_device,
        mesh=torus,
        in_specs=placed,
        out_specs=(P(SP_TP, None), P("tp", SP)),
        check_vma=False,
    )
```

profile of v0, /device:TPU:8, one launch (start us, length us, event | category | flops | bytes accessed | tf_op | source)
XLA Modules:
  0.0 314.2 jit_solution(17621082454385104322)
XLA Ops:
  8.0 0.0 all-gather.12.cloned.1.call-start
  8.0 3.9 %divide_multiply_fusion = f32[1536,512]{1,0:T(8,128)} fusion(bf16[1536,512]{1,0:T(8,128)(2,1)} %param.9, f32[512]{0:T(512)} %param.12), kind=kLoop, calls=%fused_computation.34 | loop fusion | flops 3145728 | bytes 4720640 | tf_op jit(solution)/shard_map/mul | solution.py:55
  11.9 3.1 %reshape.230 = f32[12,128,4,128]{3,2,1,0:T(4,128)S(1)} reshape(f32[1536,512]{1,0:T(8,128)} %divide_multiply_fusion) | data formatting | bytes 6291456 | tf_op jit(solution)/shard_map/reshape | solution.py:43
  15.1 0.0 copy-start
  15.1 1.7 copy-done
  16.8 2.3 negate_log-plus-one_fusion
  19.0 0.6 fusion.31
  19.7 0.2 copy.44
  19.9 3.5 %reshape.231 = bf16[12,128,4,128]{3,2,1,0:T(4,128)(2,1)} reshape(bf16[1536,512]{1,0:T(8,128)(2,1)} %param.10) | data formatting | bytes 3145728 | tf_op jit(solution)/shard_map/reshape | solution.py:43
  23.4 3.3 %fusion.15 = bf16[12,4,128,128]{3,2,1,0:T(8,128)(2,1)S(1)} fusion(f32[12,128,4,128]{3,1,2,0:T(8,128)S(1)} %fusion.31, f32[12,128,4,128]{3,2,1,0:T(4,128)} %copy-done, f32[12,4,128]{2,1,0:T(4,128)S(1)} %bitcast.247, bf16[12,128,4,128]{3,2,1,0:T(4,128)(2,1)} %reshape.231), kind=kOutput, calls=%fused_computation.23 | convolution fusion | flops 202899456 | bytes 9461760 | tf_op jit(solution)/shard_map/nshk,nshv->nhkv/dot_general | solution.py:70
  26.7 0.0 copy-start.2
  26.7 1.1 copy-done.2
  27.8 1.9 fusion
  29.7 0.0 copy-start.3
  29.7 0.0 all-gather.12.cloned.1.call-update
  29.8 0.0 all-gather.6.cloned.1.call-start
  29.8 11.2 %all_gather.29 = f32[4,4,128]{2,1,0:T(4,128)S(1)} all-gather(f32[1,4,128]{2,1,0:T(4,128)S(1)} %get-tuple-element.7), channel_id=1, replica_groups=mesh['sp_0'=8,'sp_1'=4,'sp_2'=4,'tp'=2] {'sp_2'}, dimensions={0}, use_global_device_ids=true | all-gather | bytes 10240 | tf_op jit(solution)/shard_map/all_gather | solution.py:24
  41.0 18.4 %all-gather.12.cloned.1.call-done = f32[16,128,128]{2,1,0:T(8,128)} async-done(((f32[4,128,128]{2,1,0:T(8,128)}), f32[16,128,128]{2,1,0:T(8,128)}) %all-gather.12.cloned.1.call-update) | async-done | bytes 1048592 | tf_op jit(solution)/shard_map/all_gather | solution.py:24
  59.4 2.2 bitcast_add_fusion.6
  61.7 0.0 all-gather.6.cloned.1.call-update
  61.7 0.0 all-gather.8.cloned.1.call-start
  61.7 10.9 %all_gather.30 = f32[4,4,128]{2,1,0:T(4,128)S(1)} all-gather(f32[1,4,128]{2,1,0:T(4,128)S(1)} %get-tuple-element.20), channel_id=1, replica_groups=mesh['sp_0'=8,'sp_1'=4,'sp_2'=4,'tp'=2] {'sp_1'}, dimensions={0}, use_global_device_ids=true | all-gather | bytes 10240 | tf_op jit(solution)/shard_map/all_gather | solution.py:24
  72.6 15.1 %all-gather.6.cloned.1.call-done = f32[4,4,128,128]{3,2,1,0:T(8,128)} async-done(((f32[1,4,128,128]{3,2,1,0:T(8,128)}), f32[4,4,128,128]{3,2,1,0:T(8,128)}) %all-gather.6.cloned.1.call-update) | async-done | bytes 1048592 | tf_op jit(solution)/shard_map/all_gather | solution.py:24
  87.7 2.2 multiply_add_fusion
  89.9 0.0 all-gather.8.cloned.1.call-update
  90.0 0.0 all-reduce.4.cloned.1.call-start
  90.1 24.2 %all_gather.31 = f32[8,4,128]{2,1,0:T(4,128)S(1)} all-gather(f32[1,4,128]{2,1,0:T(4,128)S(1)} %get-tuple-element.16), channel_id=1, replica_groups=mesh['sp_0'=8,'sp_1'=4,'sp_2'=4,'tp'=2] {'sp_0'}, dimensions={0}, use_global_device_ids=true | all-gather | bytes 18432 | tf_op jit(solution)/shard_map/all_gather | solution.py:24
  114.3 18.2 %all-gather.8.cloned.1.call-done = f32[8,4,128,128]{3,2,1,0:T(8,128)} async-done(((f32[1,4,128,128]{3,2,1,0:T(8,128)}), f32[8,4,128,128]{3,2,1,0:T(8,128)}) %all-gather.8.cloned.1.call-update) | async-done | bytes 2097168 | tf_op jit(solution)/shard_map/all_gather | solution.py:24
  132.5 0.0 copy-done.3
  132.5 4.6 %fusion.68 = (bf16[1,4,128,128]{3,2,1,0:T(8,128)(2,1)S(1)}, f32[4,128,128]{2,1,0:T(8,128)}) fusion(f32[4,128,128]{2,1,0:T(8,128)S(1)} %bitcast.242, f32[4,128]{1,0:T(4,128)S(1)} %fusion.80, pred[]{:T(512)S(6)} %eq.3, pred[]{:T(512)S(6)} %gt.89, pred[]{:T(512)S(6)} %gt.88, pred[]{:T(512)S(6)} %gt.87, f32[16,128,128]{2,1,0:T(8,128)} %all-gather.12.cloned.1.call-done, ...), kind=kLoop, calls=%fused_computation.84 | loop fusion | flops 3604480 | bytes 5152785
  137.1 0.8 copy.89
  137.9 0.0 all-reduce.4.cloned.1.call-update
  137.9 0.0 all-reduce.6.cloned.1.call-start
  138.0 71.2 %all-reduce.4.cloned.1.call-done = bf16[4,16384]{1,0:T(4,128)(2,1)} async-done(((bf16[4,16384]{1,0:T(4,128)(2,1)}), bf16[4,16384]{1,0:T(4,128)(2,1)}) %all-reduce.4.cloned.1.call-update) | async-done | bytes 131088 | tf_op jit(solution)/shard_map/psum | solution.py:37
  209.2 0.0 all-reduce.6.cloned.1.call-update
  209.2 0.0 all-gather.10.cloned.1.call-start
  209.3 0.5 all-gather.10.cloned.1.call-update
  209.8 0.2 all-reduce.8.cloned.1.call-start
  210.0 0.1 copy.34
  210.2 0.8 copy.36
  211.1 0.8 copy.33
  211.9 3.9 %convert_multiply_fusion = f32[1536,512]{1,0:T(8,128)} fusion(bf16[1536,512]{1,0:T(8,128)(2,1)} %param.8), kind=kLoop, calls=%fused_computation.9 | loop fusion | flops 3932160 | bytes 4718592 | tf_op jit(solution)/shard_map/jit(silu)/mul | solution.py:57
  215.8 4.9 %reshape.229 = f32[12,128,4,128]{3,2,1,0:T(4,128)} reshape(f32[1536,512]{1,0:T(8,128)} %convert_multiply_fusion) | data formatting | bytes 6291456 | tf_op jit(solution)/shard_map/reshape | solution.py:43
  220.7 4.3 %reshape.235 = f32[12,128,4,128]{3,2,1,0:T(4,128)} reshape(bf16[1536,512]{1,0:T(8,128)(2,1)} %param.11) | data formatting | bytes 4718592 | tf_op jit(solution)/shard_map/reshape | solution.py:43
  225.0 4.7 %copy.39 = f32[12,128,4,128]{1,3,2,0:T(8,128)} copy(f32[12,128,4,128]{3,2,1,0:T(4,128)} %reshape.235) | data formatting | bytes 6291456 | tf_op jit(solution)/shard_map/reshape | solution.py:43
  229.7 0.0 copy-start.1
  229.7 4.4 %bitcast_add_fusion = bf16[12,4,128,128]{3,0,2,1:T(8,128)(2,1)S(1)} fusion(f32[4,128,128]{2,1,0:T(8,128)} %get-tuple-element.3, f32[12,4,128]{0,2,1:T(8,128)} %copy.36, f32[12,4,128]{0,2,1:T(8,128)S(1)} %copy.34, f32[12,4,128]{0,2,1:T(8,128)} %copy.33, pred[12,12]{1,0:T(8,128)(4,1)S(1)} %iota_compare_fusion.2, bf16[12,4,128,128]{3,2,1,0:T(8,128)(2,1)} %copy-done.2), kind=kOutput, calls=%fused_computation.4 | convolution fusion | flops 21454848 | bytes 3481744 | tf_op jit(solution)/shard_map/jihk,ihkv->jhkv/dot_general | solution.py:78
  234.1 0.0 copy-done.1
  234.2 2.9 fusion.11
  237.1 0.0 copy-start.4
  237.1 8.2 %multiply_reduce_fusion = (f32[12,128,4]{1,2,0:T(4,128)S(1)}, f32[12,128,4,128]{1,3,2,0:T(8,128)}) fusion(f32[12,4,128,128]{3,2,1,0:T(8,128)} %fusion.11, bf16[12,128,4,128]{3,2,1,0:T(4,128)(2,1)} %reshape.231, pred[128,128]{1,0:T(8,128)(4,1)S(1)} %iota_compare_fusion, f32[12,128,4,128]{3,1,2,0:T(8,128)S(1)} %fusion.31, f32[12,128,4,128]{3,2,1,0:T(4,128)} %copy-done, ...), kind=kOutput, calls=%fused_computation.22 | convolution fusion | flops 408152064 | bytes 17342464 | tf_op jit(solution)/shard_map/nhcs,nshv->nchv/dot_general | solution.py:67
  245.3 0.0 copy-done.4
  245.3 3.9 %multiply_convert_fusion = bf16[12,128,4,128]{1,3,2,0:T(8,128)(2,1)S(1)} fusion(f32[12,128,4,128]{1,3,2,0:T(8,128)} %copy.39, f32[12,128,4,128]{1,3,2,0:T(8,128)} %get-tuple-element.25, f32[4,128]{1,0:T(4,128)S(1)} %bitcast.251, f32[12,128,4]{1,2,0:T(4,128)S(1)} %add_rsqrt_fusion), kind=kLoop, calls=%fused_computation.21 | loop fusion | flops 6291456 | bytes 7890944 | tf_op jit(solution)/shard_map/convert_element_type | solution.py:96
  249.2 1.1 copy.40
  250.3 0.6 all_to_all.14
  250.9 5.0 %all_to_all.19 = bf16[2,768,512]{2,1,0:T(8,128)(2,1)S(1)} all-to-all(bf16[2,768,512]{2,1,0:T(8,128)(2,1)S(1)} %all_to_all.14), channel_id=1, replica_groups=mesh['sp_0'=8,'sp_1'=4,'sp_2'=4,'tp'=2] {'tp'}, dimensions={0} | all-to-all | bytes 3145728 | tf_op jit(solution)/shard_map/all_to_all | solution.py:97
  255.9 0.7 copy.41
  256.6 0.0 all-reduce.6.cloned.1.call-done
  256.7 0.0 all-reduce.8.cloned.1.call-update
  256.7 0.0 all-gather.10.cloned.1.call-done
  256.7 7.0 %convolution_convert_fusion = bf16[768,2048]{1,0:T(8,128)(2,1)} fusion(bf16[768,1024]{0,1:T(8,128)(2,1)S(1)} %bitcast.240, bf16[1024,2048]{1,0:T(8,128)(2,1)} %all-gather.10.cloned.1.call-done), kind=kOutput, calls=%fused_computation.11 | convolution fusion | flops 3222798336 | bytes 8912896 | tf_op jit(solution)/shard_map/dot_general | solution.py:98
  263.7 41.8 %all-reduce.8.cloned.1.call-done = bf16[4,16384]{1,0:T(4,128)(2,1)} async-done(((bf16[4,16384]{1,0:T(4,128)(2,1)}), bf16[4,16384]{1,0:T(4,128)(2,1)}) %all-reduce.8.cloned.1.call-update) | async-done | bytes 131088 | tf_op jit(solution)/shard_map/psum | solution.py:37
  305.5 1.2 dynamic-slice_convert_fusion
  (17 shorter events, 0.2 us)
Async XLA Ops:
  8.0 51.4 %all-gather.12.cloned.1.call-start = ((), (), s32[]{:S(2)}) async-start(), calls=%async_computation.7 | async-start | bytes 1310720 | tf_op jit(solution)/shard_map/all_gather | solution.py:24
  15.1 1.7 copy-start
  26.7 1.1 copy-start.2
  29.7 102.8 %copy-start.3 = (f32[4,128,1,128]{3,2,1,0:T(1,128)S(1)}, f32[4,128,1,128]{3,2,1,0:T(1,128)}, u32[]{:S(2)}) copy-start(f32[4,128,1,128]{3,2,1,0:T(1,128)} %fusion) | copy-start | bytes 786436
  29.8 58.0 %all-gather.6.cloned.1.call-start = ((), (), s32[]{:S(2)}) async-start(), calls=%async_computation.1 | async-start | bytes 1310720 | tf_op jit(solution)/shard_map/all_gather | solution.py:24
  61.7 70.8 %all-gather.8.cloned.1.call-start = ((), (), s32[]{:S(2)}) async-start(), calls=%async_computation.2 | async-start | bytes 2359296 | tf_op jit(solution)/shard_map/all_gather | solution.py:24
  90.0 119.2 %all-reduce.4.cloned.1.call-start = ((), (), s32[]{:S(2)}) async-start(), calls=%async_computation.4 | async-start | bytes 262144 | tf_op jit(solution)/shard_map/psum | solution.py:37
  137.9 118.7 %all-reduce.6.cloned.1.call-start = ((), (), s32[]{:S(2)}) async-start(), calls=%async_computation.5 | async-start | bytes 262144 | tf_op jit(solution)/shard_map/psum | solution.py:37
  209.2 47.5 %all-gather.10.cloned.1.call-start = ((), (), s32[]{:S(2)}) async-start(), calls=%async_computation.3 | async-start | bytes 6291456 | tf_op jit(solution)/shard_map/all_gather | solution.py:100
  209.8 95.8 %all-reduce.8.cloned.1.call-start = ((), (), s32[]{:S(2)}) async-start(), calls=%async_computation.6 | async-start | bytes 262144 | tf_op jit(solution)/shard_map/psum | solution.py:37
  229.7 4.4 %copy-start.1 = (f32[12,128,4,128]{3,2,1,0:T(4,128)S(1)}, f32[12,128,4,128]{3,2,1,0:T(4,128)}, u32[]{:S(2)}) copy-start(f32[12,128,4,128]{3,2,1,0:T(4,128)} %reshape.229) | copy-start | bytes 9437188
  237.1 8.2 %copy-start.4 = (f32[512]{0:T(512)S(1)}, f32[512]{0:T(512)}, u32[]{:S(2)}) copy-start(f32[512]{0:T(512)} %param.13) | copy-start | bytes 6148
Sparse Core Ops, SparseCore 0:
  29.9 29.4 all-gather.11
  61.8 25.8 all-gather.5
  90.1 42.3 all-gather.7
  138.0 71.0 all-reduce.3
  211.3 43.8 all-reduce.5
  257.4 48.0 all-reduce.7
Sparse Core Ops, SparseCore 1:
  211.5 17.4 all-gather.9
where the time goes:
time: 315 us; the launch traced here: 314 us
  waiting for transfers between devices  165 us (52%)
  blocking collectives  51.2 us (16%)
  local copies, waits for them, and re-layouts  28.6 us (9%)
  matrix products  28.3 us (9%)
  other arithmetic  24.4 us (8%)
  between operations  15.8 us (5%)
    psum x3, waiting for transfers between devices, broadcast_by_axis(): value = lax.psum(value, axis)  113 us
    all_gather x3, waiting for transfers between devices, entering(): pieces = jax.tree.map(lambda part: lax.all_gather(part, axis), so_far)  51.7 us
    all_gather x3, blocking collectives, entering(): pieces = jax.tree.map(lambda part: lax.all_gather(part, axis), so_far)  46.2 us
    reshape x5, local copies, waits for them, and re-layouts, to_blocks(): values.reshape(blocks, BLOCK, head_count, values.shape[1] // head_count)  20.5 us
    dot_general x1, matrix products, per_device(): within = jnp.einsum('nhcs,nshv->nchv', scores, written_update)  8.21 us
    dot_general x1, matrix products, per_device(): jnp.dot(regrouped, lax.all_gather(out_weight, 'tp', axis=0, tiled=True),...  7.04 us
  transfers between devices with their start and end apart: 7, of which 5 were waited for; matrix products, arithmetic and copies ran while one was open for 15% of the time, Pallas kernels for 0%

commit v1 on v0

--- a/solution.py
+++ b/solution.py
@@ -8,6 +8,11 @@
 SP = ("sp_0", "sp_1", "sp_2")
 SP_TP = ("sp_0", "sp_1", "sp_2", "tp")
 epsilon = 1e-06
+
+
+def pieces_all_assign(along_axis, my_data):
+    current_block = lax.all_gather(my_data, along_axis).sum(axis=0)
+    return current_block
 
 
 def neutral_like(value, identity):
@@ -34,7 +39,7 @@
 def broadcast_by_axis(value, axes, root):
     value = jnp.where(lax.axis_index(axes) == root, value, jnp.zeros_like(value))
     for axis in axes:
-        value = lax.psum(value, axis)
+        value = pieces_all_assign(axis, value)
     return value
 
 

time: 315 us -> 230 us (0.73)
  waiting for transfers between devices: 165 us -> 49.1 us
  blocking collectives: 51.2 us -> 77.2 us
  other arithmetic: 24.4 us -> 28.1 us
    psum x3 -> x0, waiting for transfers between devices: 113 us -> none  [broadcast_by_axis(): value = lax.psum(value, axis)]
    all_gather x0 -> x2, blocking collectives: none -> 25.9 us  [pieces_all_assign(): current_block = lax.all_gather(my_data, along_axis).sum(axis=0)]
    all_gather x3, waiting for transfers between devices: 51.7 us -> 33.5 us  [entering(): pieces = jax.tree.map(lambda part: lax.all_gather(part, axis), so_far)]
    all_gather x0 -> x1, waiting for transfers between devices: none -> 15 us  [pieces_all_assign(): current_block = lax.all_gather(my_data, along_axis).sum(axis=0)]
    select_n x0 -> x1, other arithmetic: none -> 4.82 us  [broadcast_by_axis(): jnp.where(lax.axis_index(axes) == root, value, jnp.zeros_like(value))]
    unnamed x1 -> x0, other arithmetic: 4.63 us -> none
  transfers between devices with their start and end apart: 7 -> 5, of which waited for: 5 -> 3; matrix products, arithmetic and copies ran while one was open for 15% -> 25% of each run, Pallas kernels for 0% -> 0%
where the time goes in v1:
time: 230 us; the launch traced here: 229 us
  blocking collectives  77.2 us (34%)
  waiting for transfers between devices  49.1 us (21%)
  local copies, waits for them, and re-layouts  31.3 us (14%)
  matrix products  28.5 us (12%)
  other arithmetic  28.1 us (12%)
  between operations  14.1 us (6%)
    all_gather x3, blocking collectives, entering(): pieces = jax.tree.map(lambda part: lax.all_gather(part, axis), so_far)  46.3 us
    all_gather x3, waiting for transfers between devices, entering(): pieces = jax.tree.map(lambda part: lax.all_gather(part, axis), so_far)  33.5 us
    all_gather x2, blocking collectives, pieces_all_assign(): current_block = lax.all_gather(my_data, along_axis).sum(axis=0)  25.9 us
    reshape x5, local copies, waits for them, and re-layouts, to_blocks(): values.reshape(blocks, BLOCK, head_count, values.shape[1] // head_count)  20.6 us
    all_gather x1, waiting for transfers between devices, pieces_all_assign(): current_block = lax.all_gather(my_data, along_axis).sum(axis=0)  15 us
    dot_general x1, matrix products, per_device(): within = jnp.einsum('nhcs,nshv->nchv', scores, written_update)  8.21 us
    dot_general x1, matrix products, per_device(): jnp.dot(regrouped, lax.all_gather(out_weight, 'tp', axis=0, tiled=True),...  7.07 us
    all_to_all x1, blocking collectives, per_device(): lax.all_to_all(gated, 'tp', split_axis=0, concat_axis=1, tiled=True)  5 us
  transfers between devices with their start and end apart: 5, of which 3 were waited for; matrix products, arithmetic and copies ran while one was open for 25% of the time, Pallas kernels for 0%

profile of v1, /device:TPU:8, one launch (start us, length us, event | category | flops | bytes accessed | tf_op | source)
XLA Modules:
  0.0 228.5 jit_solution(11606101350447418665)
XLA Ops:
  7.2 0.0 all-gather.19.cloned.1.call-start
  7.2 3.9 %divide_multiply_fusion = f32[1536,512]{1,0:T(8,128)} fusion(bf16[1536,512]{1,0:T(8,128)(2,1)} %param.9, f32[512]{0:T(512)} %param.12), kind=kLoop, calls=%fused_computation.34 | loop fusion | flops 3145728 | bytes 4720640 | tf_op jit(solution)/shard_map/mul | solution.py:60
  11.1 3.1 %reshape.243 = f32[12,128,4,128]{3,2,1,0:T(4,128)S(1)} reshape(f32[1536,512]{1,0:T(8,128)} %divide_multiply_fusion) | data formatting | bytes 6291456 | tf_op jit(solution)/shard_map/reshape | solution.py:48
  14.3 0.0 copy-start
  14.3 1.7 copy-done
  16.0 2.3 negate_log-plus-one_fusion
  18.2 0.6 fusion.31
  18.9 0.9 copy.44
  19.8 3.5 %reshape.244 = bf16[12,128,4,128]{3,2,1,0:T(4,128)(2,1)} reshape(bf16[1536,512]{1,0:T(8,128)(2,1)} %param.10) | data formatting | bytes 3145728 | tf_op jit(solution)/shard_map/reshape | solution.py:48
  23.3 3.3 %fusion.15 = bf16[12,4,128,128]{3,2,1,0:T(8,128)(2,1)S(1)} fusion(f32[12,128,4,128]{3,1,2,0:T(8,128)S(1)} %fusion.31, f32[12,128,4,128]{3,2,1,0:T(4,128)} %copy-done, f32[12,4,128]{2,1,0:T(4,128)S(1)} %bitcast.245, bf16[12,128,4,128]{3,2,1,0:T(4,128)(2,1)} %reshape.244), kind=kOutput, calls=%fused_computation.23 | convolution fusion | flops 202899456 | bytes 9461760 | tf_op jit(solution)/shard_map/nshk,nshv->nhkv/dot_general | solution.py:75
  26.6 1.2 copy-done.2
  27.8 1.9 fusion
  29.7 0.0 all-gather.19.cloned.1.call-update
  29.7 0.0 all-gather.11.cloned.1.call-start
  29.7 11.2 %all_gather.45 = f32[4,4,128]{2,1,0:T(4,128)S(1)} all-gather(f32[1,4,128]{2,1,0:T(4,128)S(1)} %get-tuple-element.7), channel_id=1, replica_groups=mesh['sp_0'=8,'sp_1'=4,'sp_2'=4,'tp'=2] {'sp_2'}, dimensions={0}, use_global_device_ids=true | all-gather | bytes 10240 | tf_op jit(solution)/shard_map/all_gather | solution.py:29
  40.9 18.4 %all-gather.19.cloned.1.call-done = f32[16,128,128]{2,1,0:T(8,128)} async-done(((f32[4,128,128]{2,1,0:T(8,128)}), f32[16,128,128]{2,1,0:T(8,128)}) %all-gather.19.cloned.1.call-update) | async-done | bytes 1048592 | tf_op jit(solution)/shard_map/all_gather | solution.py:29
  59.3 2.2 bitcast_add_fusion.6
  61.6 0.0 all-gather.11.cloned.1.call-update
  61.6 0.0 all-gather.13.cloned.1.call-start
  61.6 10.9 %all_gather.46 = f32[4,4,128]{2,1,0:T(4,128)S(1)} all-gather(f32[1,4,128]{2,1,0:T(4,128)S(1)} %get-tuple-element.20), channel_id=1, replica_groups=mesh['sp_0'=8,'sp_1'=4,'sp_2'=4,'tp'=2] {'sp_1'}, dimensions={0}, use_global_device_ids=true | all-gather | bytes 10240 | tf_op jit(solution)/shard_map/all_gather | solution.py:29
  72.6 15.1 %all-gather.11.cloned.1.call-done = f32[4,4,128,128]{3,2,1,0:T(8,128)} async-done(((f32[1,4,128,128]{3,2,1,0:T(8,128)}), f32[4,4,128,128]{3,2,1,0:T(8,128)}) %all-gather.11.cloned.1.call-update) | async-done | bytes 1048592 | tf_op jit(solution)/shard_map/all_gather | solution.py:29
  87.6 2.2 multiply_add_fusion
  89.9 0.0 all-gather.13.cloned.1.call-update
  89.9 0.0 all-gather.15.cloned.1.call-start
  90.0 0.5 all-gather.15.cloned.1.call-update
  90.5 0.0 all-gather.17.cloned.1.call-start
  90.6 0.9 copy.34
  91.4 0.0 copy-done.8
  91.5 0.0 copy-done.11
  91.5 0.0 copy-done.6
  91.5 0.9 copy.36
  92.4 0.9 copy.33
  93.2 3.9 %convert_multiply_fusion = f32[1536,512]{1,0:T(8,128)} fusion(bf16[1536,512]{1,0:T(8,128)(2,1)} %param.8), kind=kLoop, calls=%fused_computation.9 | loop fusion | flops 3932160 | bytes 4718592 | tf_op jit(solution)/shard_map/jit(silu)/mul | solution.py:62
  97.1 4.9 %reshape.242 = f32[12,128,4,128]{3,2,1,0:T(4,128)} reshape(f32[1536,512]{1,0:T(8,128)} %convert_multiply_fusion) | data formatting | bytes 6291456 | tf_op jit(solution)/shard_map/reshape | solution.py:48
  102.1 4.1 %reshape.248 = f32[12,128,4,128]{3,2,1,0:T(4,128)} reshape(bf16[1536,512]{1,0:T(8,128)(2,1)} %param.11) | data formatting | bytes 4718592 | tf_op jit(solution)/shard_map/reshape | solution.py:48
  106.2 4.9 %copy.39 = f32[12,128,4,128]{1,3,2,0:T(8,128)} copy(f32[12,128,4,128]{3,2,1,0:T(4,128)} %reshape.248) | data formatting | bytes 6291456 | tf_op jit(solution)/shard_map/reshape | solution.py:48
  111.1 24.3 %all_gather.47 = f32[8,4,128]{2,1,0:T(4,128)S(1)} all-gather(f32[1,4,128]{2,1,0:T(4,128)S(1)} %get-tuple-element.16), channel_id=1, replica_groups=mesh['sp_0'=8,'sp_1'=4,'sp_2'=4,'tp'=2] {'sp_0'}, dimensions={0}, use_global_device_ids=true | all-gather | bytes 18432 | tf_op jit(solution)/shard_map/all_gather | solution.py:29
  135.4 0.6 iota_compare_fusion.2
  136.0 0.6 fusion.79
  136.6 0.6 fusion.76
  137.2 0.6 select_multiply_fusion
  137.8 0.6 slice_bitcast_fusion.8
  138.4 4.8 %fusion.67 = (bf16[4,128,128]{2,1,0:T(8,128)(2,1)S(1)}, f32[4,128,128]{2,1,0:T(8,128)}) fusion(f32[4,128,128]{2,1,0:T(8,128)S(1)} %bitcast.239, f32[4,128]{1,0:T(4,128)} %fusion.79, pred[]{:T(512)S(6)} %eq.3, pred[]{:T(512)S(6)} %gt.89, pred[]{:T(512)S(6)} %gt.88, pred[]{:T(512)S(6)} %gt.87, f32[16,128,128]{2,1,0:T(8,128)} %all-gather.19.cloned.1.call-done, ...), kind=kLoop, calls=%fused_computation.83 | loop fusion | flops 3604480 | bytes 5152785 | tf_op jit(solution)/shard_map/jit(_where)/select_n | solution.py:40
  143.2 0.7 select_n.397
  143.9 4.6 %bitcast_add_fusion = bf16[12,4,128,128]{3,0,2,1:T(8,128)(2,1)S(1)} fusion(f32[4,128,128]{2,1,0:T(8,128)} %get-tuple-element.3, f32[12,4,128]{0,2,1:T(8,128)} %copy.36, f32[12,4,128]{0,2,1:T(8,128)} %copy.34, f32[12,4,128]{0,2,1:T(8,128)} %copy.33, pred[12,12]{1,0:T(8,128)(4,1)} %iota_compare_fusion.2, bf16[12,4,128,128]{3,2,1,0:T(8,128)(2,1)} %copy-done.2), kind=kOutput, calls=%fused_computation.4 | convolution fusion | flops 21454848 | bytes 3481744 | tf_op jit(solution)/shard_map/jihk,ihkv->jhkv/dot_general | solution.py:83
  148.5 2.9 %fusion.11 = f32[12,4,128,128]{3,2,1,0:T(8,128)} fusion(bf16[12,4,128,128]{3,0,2,1:T(8,128)(2,1)S(1)} %bitcast_add_fusion, f32[12,128,4,128]{3,2,1,0:T(4,128)S(1)} %copy-done.1, f32[12,128,4,128]{3,1,2,0:T(8,128)S(1)} %fusion.31), kind=kOutput, calls=%fused_computation.16 | convolution fusion | flops 202113024 | bytes 11010048 | tf_op jit(solution)/shard_map/nchk,nhkv->nchv/dot_general | solution.py:96
  151.4 0.0 all-gather.17.cloned.1.call-update
  151.5 0.0 copy-start.13
  151.5 8.2 %multiply_reduce_fusion = (f32[12,128,4]{1,2,0:T(4,128)S(1)}, f32[12,128,4,128]{1,3,2,0:T(8,128)}) fusion(f32[12,4,128,128]{3,2,1,0:T(8,128)} %fusion.11, bf16[12,128,4,128]{3,2,1,0:T(4,128)(2,1)} %reshape.244, pred[128,128]{1,0:T(8,128)(4,1)S(1)} %iota_compare_fusion, f32[12,128,4,128]{3,1,2,0:T(8,128)S(1)} %fusion.31, f32[12,128,4,128]{3,2,1,0:T(4,128)} %copy-done, ...), kind=kOutput, calls=%fused_computation.22 | convolution fusion | flops 408152064 | bytes 17342464 | tf_op jit(solution)/shard_map/nhcs,nshv->nchv/dot_general | solution.py:72
  159.7 0.0 copy-done.13
  159.7 3.9 %multiply_convert_fusion = bf16[12,128,4,128]{1,3,2,0:T(8,128)(2,1)S(1)} fusion(f32[12,128,4,128]{1,3,2,0:T(8,128)} %copy.39, f32[12,128,4,128]{1,3,2,0:T(8,128)} %get-tuple-element.25, f32[4,128]{1,0:T(4,128)S(1)} %bitcast.249, f32[12,128,4]{1,2,0:T(4,128)S(1)} %add_rsqrt_fusion), kind=kLoop, calls=%fused_computation.21 | loop fusion | flops 6291456 | bytes 7890944 | tf_op jit(solution)/shard_map/convert_element_type | solution.py:101
  163.6 1.1 copy.40
  164.7 0.6 all_to_all.14
  165.3 5.0 %all_to_all.19 = bf16[2,768,512]{2,1,0:T(8,128)(2,1)S(1)} all-to-all(bf16[2,768,512]{2,1,0:T(8,128)(2,1)S(1)} %all_to_all.14), channel_id=1, replica_groups=mesh['sp_0'=8,'sp_1'=4,'sp_2'=4,'tp'=2] {'tp'}, dimensions={0} | all-to-all | bytes 3145728 | tf_op jit(solution)/shard_map/all_to_all | solution.py:102
  170.3 0.7 copy.41
  171.0 0.0 all-gather.15.cloned.1.call-done
  171.1 7.1 %convolution_convert_fusion = bf16[768,2048]{1,0:T(8,128)(2,1)} fusion(bf16[768,1024]{0,1:T(8,128)(2,1)S(1)} %bitcast.237, bf16[1024,2048]{1,0:T(8,128)(2,1)} %all-gather.15.cloned.1.call-done), kind=kOutput, calls=%fused_computation.11 | convolution fusion | flops 3222798336 | bytes 8912896 | tf_op jit(solution)/shard_map/dot_general | solution.py:103
  178.1 15.0 %all-gather.17.cloned.1.call-done = bf16[8,4,16384]{2,1,0:T(4,128)(2,1)} async-done(((bf16[1,4,16384]{2,1,0:T(4,128)(2,1)}), bf16[8,4,16384]{2,1,0:T(4,128)(2,1)}) %all-gather.17.cloned.1.call-update) | async-done | bytes 1048592 | tf_op jit(solution)/shard_map/all_gather | solution.py:14
  193.1 1.7 reduce_sum.46
  194.9 12.8 %all-gather.3 = bf16[4,4,16384]{2,1,0:T(4,128)(2,1)S(1)} all-gather(bf16[1,4,16384]{2,1,0:T(4,128)(2,1)S(1)} %bitcast.242), channel_id=3, replica_groups=mesh['sp_0'=8,'sp_1'=4,'sp_2'=4,'tp'=2] {'sp_1'}, dimensions={0}, use_global_device_ids=true | all-gather | bytes 655360 | tf_op jit(solution)/shard_map/all_gather | solution.py:14
  207.7 0.3 reduce_sum.47
  208.0 13.1 %all-gather.4 = bf16[4,4,16384]{2,1,0:T(4,128)(2,1)S(1)} all-gather(bf16[1,4,16384]{2,1,0:T(4,128)(2,1)S(1)} %bitcast.243), channel_id=4, replica_groups=mesh['sp_0'=8,'sp_1'=4,'sp_2'=4,'tp'=2] {'sp_2'}, dimensions={0}, use_global_device_ids=true | all-gather | bytes 655360 | tf_op jit(solution)/shard_map/all_gather | solution.py:14
  221.1 0.3 reduce_sum.48
  221.4 0.6 dynamic-slice_convert_fusion
  (33 shorter events, 0.2 us)
Async XLA Ops:
  7.2 52.2 %all-gather.19.cloned.1.call-start = ((), (), s32[]{:S(2)}) async-start(), calls=%async_computation.5 | async-start | bytes 1310720 | tf_op jit(solution)/shard_map/all_gather | solution.py:29
  14.3 1.7 copy-start
  23.3 4.5 %copy-start.4 = (bf16[12,4,128,1]{0,3,2,1:T(2,128)(2,1)S(1)}, bf16[12,4,128,1]{0,3,2,1:T(2,128)(2,1)}, u32[]{:S(2)}) copy-start(bf16[12,4,128,1]{0,3,2,1:T(2,128)(2,1)} %copy.44) | copy-start | bytes 36868
  26.6 1.2 copy-start.2
  29.7 58.0 %all-gather.11.cloned.1.call-start = ((), (), s32[]{:S(2)}) async-start(), calls=%async_computation.1 | async-start | bytes 1310720 | tf_op jit(solution)/shard_map/all_gather | solution.py:29
  40.9 31.6 %copy-start.7 = (f32[4,128]{1,0:T(4,128)}, f32[4,128]{1,0:T(4,128)S(1)}, u32[]{:S(2)}) copy-start(f32[4,128]{1,0:T(4,128)S(1)} %get-tuple-element.21) | copy-start | bytes 6148
  40.9 50.5 %copy-start.8 = (f32[4,128]{1,0:T(4,128)}, f32[4,128]{1,0:T(4,128)S(1)}, u32[]{:S(2)}) copy-start(f32[4,128]{1,0:T(4,128)S(1)} %get-tuple-element.22) | copy-start | bytes 6148
  40.9 50.5 %copy-start.9 = (f32[4,128]{1,0:T(4,128)}, f32[4,128]{1,0:T(4,128)S(1)}, u32[]{:S(2)}) copy-start(f32[4,128]{1,0:T(4,128)S(1)} %get-tuple-element.23) | copy-start | bytes 6148
  40.9 50.5 %copy-start.5 = (f32[4,128]{1,0:T(4,128)}, f32[4,128]{1,0:T(4,128)S(1)}, u32[]{:S(2)}) copy-start(f32[4,128]{1,0:T(4,128)S(1)} %bitcast_multiply_fusion) | copy-start | bytes 6148
  61.6 76.8 %all-gather.13.cloned.1.call-start = ((), (), s32[]{:S(2)}) async-start(), calls=%async_computation.2 | async-start | bytes 2359296 | tf_op jit(solution)/shard_map/all_gather | solution.py:29
  72.5 18.9 %copy-start.10 = (f32[4,128]{1,0:T(4,128)}, f32[4,128]{1,0:T(4,128)S(1)}, u32[]{:S(2)}) copy-start(f32[4,128]{1,0:T(4,128)S(1)} %get-tuple-element.17) | copy-start | bytes 6148
  72.5 18.9 %copy-start.11 = (f32[4,128]{1,0:T(4,128)}, f32[4,128]{1,0:T(4,128)S(1)}, u32[]{:S(2)}) copy-start(f32[4,128]{1,0:T(4,128)S(1)} %get-tuple-element.18) | copy-start | bytes 6148
  72.5 24.6 %copy-start.12 = (f32[4,128]{1,0:T(4,128)}, f32[4,128]{1,0:T(4,128)S(1)}, u32[]{:S(2)}) copy-start(f32[4,128]{1,0:T(4,128)S(1)} %get-tuple-element.19) | copy-start | bytes 6148
  72.6 18.9 %copy-start.6 = (f32[4,128]{1,0:T(4,128)}, f32[4,128]{1,0:T(4,128)S(1)}, u32[]{:S(2)}) copy-start(f32[4,128]{1,0:T(4,128)S(1)} %bitcast_multiply_fusion.2) | copy-start | bytes 6148
  89.9 81.2 %all-gather.15.cloned.1.call-start = ((), (), s32[]{:S(2)}) async-start(), calls=%async_computation.3 | async-start | bytes 6291456 | tf_op jit(solution)/shard_map/all_gather | solution.py:105
  90.5 102.6 %all-gather.17.cloned.1.call-start = ((), (), s32[]{:S(2)}) async-start(), calls=%async_computation.4 | async-start | bytes 1179648 | tf_op jit(solution)/shard_map/all_gather | solution.py:14
  106.2 32.3 %copy-start.3 = (f32[4,128,1,128]{3,2,1,0:T(1,128)S(1)}, f32[4,128,1,128]{3,2,1,0:T(1,128)}, u32[]{:S(2)}) copy-start(f32[4,128,1,128]{3,2,1,0:T(1,128)} %fusion) | copy-start | bytes 786436
  143.9 4.6 %copy-start.1 = (f32[12,128,4,128]{3,2,1,0:T(4,128)S(1)}, f32[12,128,4,128]{3,2,1,0:T(4,128)}, u32[]{:S(2)}) copy-start(f32[12,128,4,128]{3,2,1,0:T(4,128)} %reshape.242) | copy-start | bytes 9437188
  151.5 8.2 %copy-start.13 = (f32[512]{0:T(512)S(1)}, f32[512]{0:T(512)}, u32[]{:S(2)}) copy-start(f32[512]{0:T(512)} %param.13) | copy-start | bytes 6148
Sparse Core Ops, SparseCore 0:
  29.8 29.4 all-gather.18
  61.7 25.8 all-gather.10
  90.0 42.4 all-gather.12
  134.2 17.5 all-gather.14
  153.4 39.7 all-gather.16
